TPU v7x, 32 devices: a whole 2x2x4 slice. The times are simulated.
32 devices in a mesh: fs: 4 (over y, x), tp: 8 (over z, core).
Axes of the slice: x: 2, y: 2, z: 4, core: 2. Of those that a mesh axis runs over, the one named last changes fastest.
Arguments:
- tokens: bfloat16 [2048, 2048], P('fs', 'tp'), may hold values from -6 to 6
- norm_gain: float32 [2048], P('fs'), may hold values from 0.1 to 1.9
- gate_train: float32 [2048, 8192], P('fs', 'tp'), may hold values from -0.125 to 0.125
- up_train: float32 [2048, 8192], P('fs', 'tp'), may hold values from -0.125 to 0.125
- down_train: float32 [8192, 2048], P('fs', 'tp'), may hold values from -0.0625 to 0.0625
Outputs:
- gate_serve: bfloat16 [2048, 8192], P(None, 'tp')
- up_serve: bfloat16 [2048, 8192], P(None, 'tp')
- down_serve: bfloat16 [8192, 2048], P('tp')
- layer_out: bfloat16 [2048, 2048], P(('fs', 'tp'))
All inputs are finite; a program needn't handle non-finite values.
Results may differ from a plain program's by a relative error of at most 0.024.
Values may be sent and summed in bfloat16 or wider, within the bound.
A program may use at most 64 MiB of HBM per device.

v0:
```python
import jax
import jax.numpy as jnp
from jax import lax
from jax.sharding import PartitionSpec as P

D = 2048
epsilon = 1e-06


def body(tokens, norm_gain, gate_train, up_train, down_train):
    gate_local = (norm_gain[:, None] * gate_train).astype(jnp.bfloat16)
    up_local = (norm_gain[:, None] * up_train).astype(jnp.bfloat16)
    down_local = down_train.astype(jnp.bfloat16)
    features = lax.all_gather(tokens, "tp", axis=1, tiled=True)
    wide = features.astype(jnp.float32)
    squares = jnp.sum(wide * wide, axis=1)
    gate_whole, up_whole = (
        lax.all_gather(gate_local, "fs", axis=0, tiled=True),
        lax.all_gather(up_local, "fs", axis=0, tiled=True),
    )
    gate_sum = jnp.dot(features, gate_whole, preferred_element_type=jnp.float32)
    up_sum = jnp.dot(features, up_whole, preferred_element_type=jnp.float32)
    down_rows = lax.all_gather(down_local, "fs", axis=0, tiled=True)
    down_whole = lax.all_to_all(down_rows, "tp", split_axis=0, concat_axis=1, tiled=True)
    scale = lax.rsqrt(squares / D + epsilon)[:, None]
    hidden = (jax.nn.silu(gate_sum * scale) * (up_sum * scale)).astype(jnp.bfloat16)
    mixed = lax.psum_scatter(
        jnp.dot(hidden, down_whole, preferred_element_type=jnp.float32).astype(jnp.bfloat16),
        "tp",
        scatter_dimension=0,
        tiled=True,
    )
    return (gate_whole, up_whole, down_whole, mixed)


def solution(mesh):
    return jax.shard_map(
        body,
        mesh=mesh,
        in_specs=(P("fs", "tp"), P("fs"), P("fs", "tp"), P("fs", "tp"), P("fs", "tp")),
        out_specs=(P(None, "tp"), P(None, "tp"), P("tp", None), P(("fs", "tp"), None)),
        check_vma=False,
    )
```

profile of v0, /device:TPU:0, one launch (start us, length us, event | category | flops | bytes accessed | tf_op | source)
XLA Modules:
  0.0 293.7 jit_solution(2137613969868247611)
XLA Ops:
  7.2 0.0 copy-start.2
  7.2 0.0 copy-start.3
  7.2 0.0 all-gather.9.cloned.1.call-start
  7.2 2.8 convert_element_type.20
  10.0 0.0 all-gather.9.cloned.1.call-update
  10.1 0.0 all-gather.11.cloned.1.call-start
  10.1 0.7 all-gather.11.cloned.1.call-update
  10.8 0.0 all-gather.5.cloned.1.call-start
  10.9 0.0 copy-done.2
  10.9 0.0 copy-done.3
  10.9 3.2 %multiply_convert_fusion = (bf16[512,1024]{1,0:T(8,128)(2,1)}, bf16[512,1024]{1,0:T(8,128)(2,1)}) fusion(f32[512,1024]{1,0:T(8,128)S(1)} %copy-done.2, f32[512]{0:T(512)S(1)} %copy-done.3, f32[512,1024]{1,0:T(8,128)} %param.7), kind=kLoop, calls=%fused_computation.9 | loop fusion | flops 2097152 | bytes 6293504 | tf_op jit(solution)/shard_map/convert_element_type | solution.py:12
  14.1 0.0 all-gather.5.cloned.1.call-update
  14.1 51.6 %all-gather.9.cloned.1.call-done = bf16[8192,256]{1,0:T(8,128)(2,1)} async-done(((bf16[2048,256]{1,0:T(8,128)(2,1)}), bf16[8192,256]{1,0:T(8,128)(2,1)}) %all-gather.9.cloned.1.call-update) | async-done | bytes 4194320 | tf_op jit(solution)/shard_map/all_gather | solution.py:23
  65.7 4.6 %all-to-all-start = ((bf16[8,1024,256]{2,1,0:T(8,128)(2,1)}), bf16[8,1024,256]{2,1,0:T(8,128)(2,1)}, u32[]{:S(2)}, u32[]{:S(2)}) async-start(bf16[8,1024,256]{2,1,0:T(8,128)(2,1)} %bitcast.32), calls=%async_computation | async-start | bytes 8388608 | tf_op jit(solution)/shard_map/all_to_all | solution.py:24
  70.3 0.0 all-gather.7.cloned.1.call-start
  70.4 0.5 all-gather.7.cloned.1.call-update
  70.9 0.0 reduce-scatter.2.cloned.1.call-start
  71.0 50.9 %all-gather.11.cloned.1.call-done = bf16[512,2048]{1,0:T(8,128)(2,1)} async-done(((bf16[512,256]{1,0:T(8,128)(2,1)}), bf16[512,2048]{1,0:T(8,128)(2,1)}) %all-gather.11.cloned.1.call-update) | async-done | bytes 2097168 | tf_op jit(solution)/shard_map/all_gather | solution.py:14
  121.8 0.0 copy-start.1
  121.8 2.2 multiply_reduce_fusion
  124.1 54.8 %all-gather.5.cloned.1.call-done = bf16[2048,1024]{1,0:T(8,128)(2,1)} async-done(((bf16[512,1024]{1,0:T(8,128)(2,1)}), bf16[2048,1024]{1,0:T(8,128)(2,1)}) %all-gather.5.cloned.1.call-update) | async-done | bytes 4194320 | tf_op jit(solution)/shard_map/all_gather | solution.py:18
  178.9 0.0 copy-done.1
  178.9 5.9 %fusion.5 = f32[1024,512]{1,0:T(8,128)} fusion(bf16[2048,1024]{1,0:T(8,128)(2,1)} %all-gather.5.cloned.1.call-done, bf16[512,2048]{1,0:T(8,128)(2,1)S(1)} %copy-done.1), kind=kOutput, calls=%fused_computation.13 | convolution fusion | flops 2147483648 | bytes 8388608 | tf_op jit(solution)/shard_map/dot_general | solution.py:21
  184.8 0.0 all-to-all-done
  184.8 6.5 %copy.10 = bf16[8,1024,256]{1,2,0:T(8,128)(2,1)} copy(bf16[8,1024,256]{2,1,0:T(8,128)(2,1)} %all-to-all-done) | data formatting | bytes 8388608 | tf_op jit(solution)/shard_map/all_to_all | solution.py:24
  191.2 42.5 %all-gather.7.cloned.1.call-done = bf16[2048,1024]{1,0:T(8,128)(2,1)} async-done(((bf16[512,1024]{1,0:T(8,128)(2,1)}), bf16[2048,1024]{1,0:T(8,128)(2,1)}) %all-gather.7.cloned.1.call-update) | async-done | bytes 4194320 | tf_op jit(solution)/shard_map/all_gather | solution.py:19
  233.7 10.3 %convolution_convert_fusion = bf16[512,2048]{1,0:T(8,128)(2,1)} fusion(bf16[1024,2048]{0,1:T(8,128)(2,1)} %bitcast.30, f32[1024,512]{1,0:T(8,128)} %fusion.5, bf16[2048,1024]{1,0:T(8,128)(2,1)} %all-gather.7.cloned.1.call-done, bf16[512,2048]{1,0:T(8,128)(2,1)S(1)} %copy-done.1, f32[512]{0:T(512)S(1)} %add_rsqrt_fusion), kind=kOutput, calls=%fused_computation.1 | convolution fusion | flops 4300210176 | bytes 14682112 | tf_op jit(solution)/shard_map/dot_general | solution.py:28
  244.0 0.0 reduce-scatter.2.cloned.1.call-update
  244.0 6.4 %copy.11 = bf16[1024,2048]{1,0:T(8,128)(2,1)} copy(bf16[1024,2048]{0,1:T(8,128)(2,1)} %bitcast.31) | data formatting | bytes 8388608
  250.5 29.8 %reduce-scatter.2.cloned.1.call-done = bf16[64,2048]{1,0:T(8,128)(2,1)} async-done(((bf16[512,2048]{1,0:T(8,128)(2,1)}), bf16[64,2048]{1,0:T(8,128)(2,1)}) %reduce-scatter.2.cloned.1.call-update) | async-done | bytes 262160 | tf_op jit(solution)/shard_map/reduce_scatter | solution.py:27
  280.3 0.0 copy-start
  280.3 4.8 %copy.14 = bf16[2048,1024]{1,0:T(8,128)(2,1)} copy(bf16[2048,1024]{1,0:T(8,128)(2,1)} %all-gather.5.cloned.1.call-done) | data formatting | bytes 8388608
  285.1 0.0 copy-done
  285.1 2.0 copy.15
  (1 shorter events, 0.0 us)
Async XLA Ops:
  7.2 3.7 %copy-start.2 = (f32[512,1024]{1,0:T(8,128)S(1)}, f32[512,1024]{1,0:T(8,128)}, u32[]{:S(2)}) copy-start(f32[512,1024]{1,0:T(8,128)} %param.8) | copy-start | bytes 6291460
  7.2 3.7 %copy-start.3 = (f32[512]{0:T(512)S(1)}, f32[512]{0:T(512)}, u32[]{:S(2)}) copy-start(f32[512]{0:T(512)} %param.6) | copy-start | bytes 6148
  7.2 58.6 %all-gather.9.cloned.1.call-start = ((), (), s32[]{:S(2)}) async-start(), calls=%async_computation.4 | async-start | bytes 5242880 | tf_op jit(solution)/shard_map/all_gather | solution.py:23
  10.1 111.8 %all-gather.11.cloned.1.call-start = ((), (), s32[]{:S(2)}) async-start(), calls=%async_computation.5 | async-start | bytes 2359296 | tf_op jit(solution)/shard_map/all_gather | solution.py:14
  10.8 168.1 %all-gather.5.cloned.1.call-start = ((), (), s32[]{:S(2)}) async-start(), calls=%async_computation.2 | async-start | bytes 5242880 | tf_op jit(solution)/shard_map/all_gather | solution.py:18
  65.7 119.0 %all-to-all-start = ((bf16[8,1024,256]{2,1,0:T(8,128)(2,1)}), bf16[8,1024,256]{2,1,0:T(8,128)(2,1)}, u32[]{:S(2)}, u32[]{:S(2)}) async-start(bf16[8,1024,256]{2,1,0:T(8,128)(2,1)} %bitcast.32), calls=%async_computation | async-start | bytes 8388608 | tf_op jit(solution)/shard_map/all_to_all | solution.py:24
  70.3 163.4 %all-gather.7.cloned.1.call-start = ((), (), s32[]{:S(2)}) async-start(), calls=%async_computation.3 | async-start | bytes 5242880 | tf_op jit(solution)/shard_map/all_gather | solution.py:19
  70.9 209.4 %reduce-scatter.2.cloned.1.call-start = ((), (), s32[]{:S(2)}) async-start(), calls=%async_computation.6 | async-start | bytes 2359296 | tf_op jit(solution)/shard_map/reduce_scatter | solution.py:27
  121.8 57.0 %copy-start.1 = (bf16[512,2048]{1,0:T(8,128)(2,1)S(1)}, bf16[512,2048]{1,0:T(8,128)(2,1)}, u32[]{:S(2)}) copy-start(bf16[512,2048]{1,0:T(8,128)(2,1)} %all-gather.11.cloned.1.call-done) | copy-start | bytes 6291460
  280.3 4.8 %copy-start = (bf16[2048,1024]{1,0:T(8,128)(2,1)S(1)}, bf16[2048,1024]{1,0:T(8,128)(2,1)}, u32[]{:S(2)}) copy-start(bf16[2048,1024]{1,0:T(8,128)(2,1)} %all-gather.7.cloned.1.call-done) | copy-start | bytes 12582916
Sparse Core Ops, SparseCore 0:
  10.4 55.2 all-gather.8
  67.3 54.4 all-gather.10
  124.3 54.5 all-gather.4
  181.1 52.5 all-gather.6
  244.2 36.0 reduce-scatter.1
where the time goes:
time: 294 us
  waiting for transfers between devices  231 us (79%)
  local copies, waits for them, and re-layouts  19.8 us (7%)
  matrix products  16.2 us (6%)
  between operations  13.8 us (5%)
  other arithmetic  8.23 us (3%)
  starting transfers between devices  4.8 us (2%)
    all_gather x1, waiting for transfers between devices, body(): lax.all_gather(gate_local, 'fs', axis=0, tiled=True)  54.8 us
    all_gather x1, waiting for transfers between devices, body(): down_rows = lax.all_gather(down_local, 'fs', axis=0, tiled=True)  51.6 us
    all_gather x1, waiting for transfers between devices, body(): features = lax.all_gather(tokens, 'tp', axis=1, tiled=True)  50.9 us
    all_gather x1, waiting for transfers between devices, body(): lax.all_gather(up_local, 'fs', axis=0, tiled=True)  42.5 us
    reduce_scatter x1, waiting for transfers between devices, body(): lax.psum_scatter(jnp.dot(hidden, down_whole, preferred_element_type=jnp.f...  29.8 us
    unnamed x11, local copies, waits for them, and re-layouts  13.3 us
    dot_general x1, matrix products, body(): jnp.dot(hidden, down_whole, preferred_element_type=jnp.float32)  10.3 us
    all_to_all x1, local copies, waits for them, and re-layouts, body(): lax.all_to_all(down_rows, 'tp', split_axis=0, concat_axis=1, tiled=True)  6.48 us
  transfers between devices with their start and end apart: 6, of which 5 were waited for; matrix products, arithmetic and copies ran while one was open for 8% of the time, Pallas kernels for 0%

commit v1 on v0

--- a/solution.py
+++ b/solution.py
@@ -11,7 +11,16 @@
     gate_local = (norm_gain[:, None] * gate_train).astype(jnp.bfloat16)
     up_local = (norm_gain[:, None] * up_train).astype(jnp.bfloat16)
     down_local = down_train.astype(jnp.bfloat16)
-    features = lax.all_gather(tokens, "tp", axis=1, tiled=True)
+    size, index, width = (lax.axis_size("tp"), lax.axis_index("tp"), tokens.shape[1])
+    forward = [(i, (i + 1) % size) for i in range(size)]
+    whole = jnp.zeros((*tokens.shape[:1], size * width, *tokens.shape[1 + 1 :]), tokens.dtype)
+    block = tokens
+    for hop in range(size):
+        source = (index - hop) % size
+        whole = lax.dynamic_update_slice_in_dim(whole, block, source * width, axis=1)
+        if hop < size - 1:
+            block = lax.ppermute(block, "tp", forward)
+    features = whole
     wide = features.astype(jnp.float32)
     squares = jnp.sum(wide * wide, axis=1)
     gate_whole, up_whole = (

time: 294 us -> 272 us (0.925)
  waiting for transfers between devices: 231 us -> 193 us
  starting transfers between devices: 4.8 us -> 22.6 us
    ppermute x0 -> x7, waiting for transfers between devices: none -> 105 us  [body(): block = lax.ppermute(block, 'tp', forward)]
    all_gather x1, waiting for transfers between devices: 54.8 us -> 0.02 us  [body(): lax.all_gather(gate_local, 'fs', axis=0, tiled=True)]
    all_gather x1 -> x0, waiting for transfers between devices: 50.9 us -> none  [body(): features = lax.all_gather(tokens, 'tp', axis=1, tiled=True)]
    all_gather x1, waiting for transfers between devices: 42.5 us -> 0.01 us  [body(): lax.all_gather(up_local, 'fs', axis=0, tiled=True)]
    ppermute x0 -> x7, starting transfers between devices: none -> 17.7 us  [body(): block = lax.ppermute(block, 'tp', forward)]
    reduce_scatter x1, waiting for transfers between devices: 29.8 us -> 34.2 us  [body(): lax.psum_scatter(jnp.dot(hidden, down_whole, preferred_element_type=jnp.f...]
    unnamed x11 -> x15, local copies, waits for them, and re-layouts: 13.3 us -> 13.3 us
  transfers between devices with their start and end apart: 6 -> 12, of which waited for: 5 -> 9; matrix products, arithmetic and copies ran while one was open for 8% -> 8% of each run, Pallas kernels for 0% -> 0%
where the time goes in v1:
time: 272 us
  waiting for transfers between devices  193 us (71%)
  starting transfers between devices  22.6 us (8%)
  local copies, waits for them, and re-layouts  20.2 us (7%)
  matrix products  15.9 us (6%)
  between operations  13.9 us (5%)
  other arithmetic  6.5 us (2%)
    ppermute x7, waiting for transfers between devices, body(): block = lax.ppermute(block, 'tp', forward)  105 us
    all_gather x1, waiting for transfers between devices, body(): down_rows = lax.all_gather(down_local, 'fs', axis=0, tiled=True)  52.4 us
    reduce_scatter x1, waiting for transfers between devices, body(): lax.psum_scatter(jnp.dot(hidden, down_whole, preferred_element_type=jnp.f...  34.2 us
    ppermute x7, starting transfers between devices, body(): block = lax.ppermute(block, 'tp', forward)  17.7 us
    unnamed x15, local copies, waits for them, and re-layouts  13.3 us
    dot_general x1, matrix products, body(): jnp.dot(hidden, down_whole, preferred_element_type=jnp.float32)  10.1 us
    all_to_all x1, local copies, waits for them, and re-layouts, body(): lax.all_to_all(down_rows, 'tp', split_axis=0, concat_axis=1, tiled=True)  6.43 us
    dot_general x1, matrix products, body(): gate_sum = jnp.dot(features, gate_whole, preferred_element_type=jnp.float32)  5.84 us
  transfers between devices with their start and end apart: 12, of which 9 were waited for; matrix products, arithmetic and copies ran while one was open for 8% of the time, Pallas kernels for 0%

profile of v1, /device:TPU:0, one launch (start us, length us, event | category | flops | bytes accessed | tf_op | source)
XLA Modules:
  0.0 271.6 jit_solution(8709022535425657729)
XLA Ops:
  7.2 0.0 copy-start.1
  7.2 0.0 copy-start.5
  7.2 0.0 all-gather.8.cloned.1.call-start
  7.2 2.8 %convert_element_type.20 = bf16[2048,256]{1,0:T(8,128)(2,1)} convert(f32[2048,256]{1,0:T(8,128)} %param.9) | non-fusion elementwise | flops 524288 | bytes 3145728 | tf_op jit(solution)/shard_map/convert_element_type | solution.py:13
  10.0 0.0 all-gather.8.cloned.1.call-update
  10.1 0.0 all-gather.4.cloned.1.call-start
  10.1 0.0 copy-done.1
  10.1 0.0 copy-done.5
  10.1 3.2 %multiply_convert_fusion.1 = (bf16[512,1024]{1,0:T(8,128)(2,1)}, bf16[512,1024]{1,0:T(8,128)(2,1)}) fusion(f32[512,1024]{1,0:T(8,128)S(1)} %copy-done.1, f32[512]{0:T(512)S(1)} %copy-done.5, f32[512,1024]{1,0:T(8,128)} %param.7), kind=kLoop, calls=%fused_computation.3 | loop fusion | flops 2097152 | bytes 6293504 | tf_op jit(solution)/shard_map/convert_element_type | solution.py:12
  13.3 0.0 all-gather.4.cloned.1.call-update
  13.4 52.4 %all-gather.8.cloned.1.call-done = bf16[8192,256]{1,0:T(8,128)(2,1)} async-done(((bf16[2048,256]{1,0:T(8,128)(2,1)}), bf16[8192,256]{1,0:T(8,128)(2,1)}) %all-gather.8.cloned.1.call-update) | async-done | bytes 4194320 | tf_op jit(solution)/shard_map/all_gather | solution.py:32
  65.7 0.0 copy-start.2
  65.7 4.7 %all-to-all-start = ((bf16[8,1024,256]{2,1,0:T(8,128)(2,1)}), bf16[8,1024,256]{2,1,0:T(8,128)(2,1)}, u32[]{:S(2)}, u32[]{:S(2)}) async-start(bf16[8,1024,256]{2,1,0:T(8,128)(2,1)} %bitcast.11), calls=%async_computation | async-start | bytes 8388608 | tf_op jit(solution)/shard_map/all_to_all | solution.py:33
  70.5 0.0 all-gather.6.cloned.1.call-start
  70.5 0.7 all-gather.6.cloned.1.call-update
  71.2 0.0 reduce-scatter.2.cloned.1.call-start
  71.3 0.0 copy-done.2
  71.3 0.5 collective-permute-start
  71.8 74.0 %collective-permute-done = bf16[512,256]{1,0:T(8,128)(2,1)S(1)} collective-permute-done((bf16[512,256]{1,0:T(8,128)(2,1)S(1)}, bf16[512,256]{1,0:T(8,128)(2,1)S(1)}, u32[]{:S(2)}, u32[]{:S(2)}) %collective-permute-start) | collective-permute-done | bytes 262176 | tf_op jit(solution)/shard_map/ppermute | solution.py:22
  145.8 0.0 collective-permute-start.1
  145.8 7.7 %collective-permute-done.1 = bf16[512,256]{1,0:T(8,128)(2,1)S(1)} collective-permute-done((bf16[512,256]{1,0:T(8,128)(2,1)S(1)}, bf16[512,256]{1,0:T(8,128)(2,1)S(1)}, u32[]{:S(2)}, u32[]{:S(2)}) %collective-permute-start.1) | collective-permute-done | bytes 262176 | tf_op jit(solution)/shard_map/ppermute | solution.py:22
  153.5 0.0 collective-permute-start.2
  153.5 7.7 %collective-permute-done.2 = bf16[512,256]{1,0:T(8,128)(2,1)S(1)} collective-permute-done((bf16[512,256]{1,0:T(8,128)(2,1)S(1)}, bf16[512,256]{1,0:T(8,128)(2,1)S(1)}, u32[]{:S(2)}, u32[]{:S(2)}) %collective-permute-start.2) | collective-permute-done | bytes 262176 | tf_op jit(solution)/shard_map/ppermute | solution.py:22
  161.2 0.0 copy-start.3
  161.2 9.2 %collective-permute-start.3 = (bf16[512,256]{1,0:T(8,128)(2,1)S(1)}, bf16[512,256]{1,0:T(8,128)(2,1)S(1)}, u32[]{:S(2)}, u32[]{:S(2)}) collective-permute-start(bf16[512,256]{1,0:T(8,128)(2,1)S(1)} %collective-permute-done.2), channel_id=1, source_target_pairs={{0,1},{1,2},{2,3},{3,4},{4,5},{5,6},{6,7},{7,0},{8,9},{9,10},{10,1... | collective-permute-start | bytes 786440 | tf_op jit(solution)/shard_map/ppermute | solution.py:22
  170.5 1.2 collective-permute-done.3
  171.6 0.0 copy-done.3
  171.6 4.6 %collective-permute-start.4 = (bf16[512,256]{1,0:T(8,128)(2,1)S(1)}, bf16[512,256]{1,0:T(8,128)(2,1)S(1)}, u32[]{:S(2)}, u32[]{:S(2)}) collective-permute-start(bf16[512,256]{1,0:T(8,128)(2,1)S(1)} %collective-permute-done.3), channel_id=1, source_target_pairs={{0,1},{1,2},{2,3},{3,4},{4,5},{5,6},{6,7},{7,0},{8,9},{9,10},{10,1... | collective-permute-start | bytes 786440 | tf_op jit(solution)/shard_map/ppermute | solution.py:22
  176.3 0.0 copy-start.4
  176.3 0.2 broadcast_in_dim.2
  176.5 3.0 %collective-permute-done.4 = bf16[512,256]{1,0:T(8,128)(2,1)S(1)} collective-permute-done((bf16[512,256]{1,0:T(8,128)(2,1)S(1)}, bf16[512,256]{1,0:T(8,128)(2,1)S(1)}, u32[]{:S(2)}, u32[]{:S(2)}) %collective-permute-start.4) | collective-permute-done | bytes 262176 | tf_op jit(solution)/shard_map/ppermute | solution.py:22
  179.5 2.5 collective-permute-start.5
  182.1 0.0 copy-done.4
  182.2 4.9 %collective-permute-done.5 = bf16[512,256]{1,0:T(8,128)(2,1)S(1)} collective-permute-done((bf16[512,256]{1,0:T(8,128)(2,1)S(1)}, bf16[512,256]{1,0:T(8,128)(2,1)S(1)}, u32[]{:S(2)}, u32[]{:S(2)}) %collective-permute-start.5) | collective-permute-done | bytes 262176 | tf_op jit(solution)/shard_map/ppermute | solution.py:22
  187.1 0.7 collective-permute-start.6
  188.0 6.8 %collective-permute-done.6 = bf16[512,256]{1,0:T(8,128)(2,1)S(1)} collective-permute-done((bf16[512,256]{1,0:T(8,128)(2,1)S(1)}, bf16[512,256]{1,0:T(8,128)(2,1)S(1)}, u32[]{:S(2)}, u32[]{:S(2)}) %collective-permute-start.6) | collective-permute-done | bytes 262176 | tf_op jit(solution)/shard_map/ppermute | solution.py:22
  194.7 0.5 multiply_reduce_fusion
  195.2 0.0 all-gather.4.cloned.1.call-done
  195.3 5.8 %fusion.1 = f32[512,1024]{1,0:T(8,128)} fusion(bf16[512,2048]{1,0:T(8,128)(2,1)S(1)} %constant_dynamic-update-slice_fusion, bf16[2048,1024]{1,0:T(8,128)(2,1)} %all-gather.4.cloned.1.call-done), kind=kOutput, calls=%fused_computation.15 | convolution fusion | flops 2147483648 | bytes 8388608 | tf_op jit(solution)/shard_map/dot_general | solution.py:30
  201.1 0.0 all-to-all-done
  201.1 6.4 %copy.10 = bf16[8,1024,256]{1,2,0:T(8,128)(2,1)} copy(bf16[8,1024,256]{2,1,0:T(8,128)(2,1)} %all-to-all-done) | data formatting | bytes 8388608 | tf_op jit(solution)/shard_map/all_to_all | solution.py:33
  207.5 10.1 %convolution_convert_fusion = bf16[512,2048]{1,0:T(8,128)(2,1)} fusion(bf16[1024,2048]{0,1:T(8,128)(2,1)} %bitcast.9, f32[512,1024]{1,0:T(8,128)} %fusion.1, bf16[512,2048]{1,0:T(8,128)(2,1)S(1)} %constant_dynamic-update-slice_fusion, bf16[2048,1024]{1,0:T(8,128)(2,1)} %all-gather.6.cloned.1.call-done, f32[512]{0:T(512)S(1)} %add_rsqrt_fusion), kind=kOutput, calls=%fused_computation.1 | convolution fusion | flops 4300210176 | bytes 14682112 | tf_op jit(solution)/shard_map/dot_general | solution.py:37
  217.6 0.0 reduce-scatter.2.cloned.1.call-update
  217.6 6.4 %copy.11 = bf16[1024,2048]{1,0:T(8,128)(2,1)} copy(bf16[1024,2048]{0,1:T(8,128)(2,1)} %bitcast.10) | data formatting | bytes 8388608
  224.1 34.2 %reduce-scatter.2.cloned.1.call-done = bf16[64,2048]{1,0:T(8,128)(2,1)} async-done(((bf16[512,2048]{1,0:T(8,128)(2,1)}), bf16[64,2048]{1,0:T(8,128)(2,1)}) %reduce-scatter.2.cloned.1.call-update) | async-done | bytes 262160 | tf_op jit(solution)/shard_map/reduce_scatter | solution.py:36
  258.3 4.8 %copy.22 = bf16[2048,1024]{1,0:T(8,128)(2,1)} copy(bf16[2048,1024]{1,0:T(8,128)(2,1)} %all-gather.4.cloned.1.call-done) | data formatting | bytes 8388608
  263.1 0.0 copy-done
  263.1 2.0 copy.23
  (11 shorter events, 0.2 us)
Async XLA Ops:
  7.2 2.9 %copy-start.1 = (f32[512,1024]{1,0:T(8,128)S(1)}, f32[512,1024]{1,0:T(8,128)}, u32[]{:S(2)}) copy-start(f32[512,1024]{1,0:T(8,128)} %param.8) | copy-start | bytes 6291460
  7.2 2.9 %copy-start.5 = (f32[512]{0:T(512)S(1)}, f32[512]{0:T(512)}, u32[]{:S(2)}) copy-start(f32[512]{0:T(512)} %param.6) | copy-start | bytes 6148
  7.2 58.6 %all-gather.8.cloned.1.call-start = ((), (), s32[]{:S(2)}) async-start(), calls=%async_computation.4 | async-start | bytes 5242880 | tf_op jit(solution)/shard_map/all_gather | solution.py:32
  10.1 185.2 %all-gather.4.cloned.1.call-start = ((), (), s32[]{:S(2)}) async-start(), calls=%async_computation.2 | async-start | bytes 5242880 | tf_op jit(solution)/shard_map/all_gather | solution.py:27
  65.7 5.5 %copy-start.2 = (bf16[512,256]{1,0:T(8,128)(2,1)S(1)}, bf16[512,256]{1,0:T(8,128)(2,1)}, u32[]{:S(2)}) copy-start(bf16[512,256]{1,0:T(8,128)(2,1)} %param.5) | copy-start | bytes 786436
  65.7 135.4 %all-to-all-start = ((bf16[8,1024,256]{2,1,0:T(8,128)(2,1)}), bf16[8,1024,256]{2,1,0:T(8,128)(2,1)}, u32[]{:S(2)}, u32[]{:S(2)}) async-start(bf16[8,1024,256]{2,1,0:T(8,128)(2,1)} %bitcast.11), calls=%async_computation | async-start | bytes 8388608 | tf_op jit(solution)/shard_map/all_to_all | solution.py:33
  70.5 137.1 %all-gather.6.cloned.1.call-start = ((), (), s32[]{:S(2)}) async-start(), calls=%async_computation.3 | async-start | bytes 5242880 | tf_op jit(solution)/shard_map/all_gather | solution.py:28
  71.2 187.1 %reduce-scatter.2.cloned.1.call-start = ((), (), s32[]{:S(2)}) async-start(), calls=%async_computation.5 | async-start | bytes 2359296 | tf_op jit(solution)/shard_map/reduce_scatter | solution.py:36
  71.3 74.6 %collective-permute-start = (bf16[512,256]{1,0:T(8,128)(2,1)S(1)}, bf16[512,256]{1,0:T(8,128)(2,1)S(1)}, u32[]{:S(2)}, u32[]{:S(2)}) collective-permute-start(bf16[512,256]{1,0:T(8,128)(2,1)S(1)} %copy-done.2), channel_id=1, source_target_pairs={{0,1},{1,2},{2,3},{3,4},{4,5},{5,6},{6,7},{7,0},{8,9},{9,10},{10,1... | collective-permute-start | bytes 786440 | tf_op jit(solution)/shard_map/ppermute | solution.py:22
  145.8 7.7 %collective-permute-start.1 = (bf16[512,256]{1,0:T(8,128)(2,1)S(1)}, bf16[512,256]{1,0:T(8,128)(2,1)S(1)}, u32[]{:S(2)}, u32[]{:S(2)}) collective-permute-start(bf16[512,256]{1,0:T(8,128)(2,1)S(1)} %collective-permute-done), channel_id=1, source_target_pairs={{0,1},{1,2},{2,3},{3,4},{4,5},{5,6},{6,7},{7,0},{8,9},{9,10},{10,1... | collective-permute-start | bytes 786440 | tf_op jit(solution)/shard_map/ppermute | solution.py:22
  153.5 7.7 %collective-permute-start.2 = (bf16[512,256]{1,0:T(8,128)(2,1)S(1)}, bf16[512,256]{1,0:T(8,128)(2,1)S(1)}, u32[]{:S(2)}, u32[]{:S(2)}) collective-permute-start(bf16[512,256]{1,0:T(8,128)(2,1)S(1)} %collective-permute-done.1), channel_id=1, source_target_pairs={{0,1},{1,2},{2,3},{3,4},{4,5},{5,6},{6,7},{7,0},{8,9},{9,10},{10,1... | collective-permute-start | bytes 786440 | tf_op jit(solution)/shard_map/ppermute | solution.py:22
  161.2 10.4 %copy-start.3 = (bf16[512,256]{1,0:T(8,128)(2,1)}, bf16[512,256]{1,0:T(8,128)(2,1)S(1)}, u32[]{:S(2)}) copy-start(bf16[512,256]{1,0:T(8,128)(2,1)S(1)} %collective-permute-done.2) | copy-start | bytes 786436
  161.2 10.4 %collective-permute-start.3 = (bf16[512,256]{1,0:T(8,128)(2,1)S(1)}, bf16[512,256]{1,0:T(8,128)(2,1)S(1)}, u32[]{:S(2)}, u32[]{:S(2)}) collective-permute-start(bf16[512,256]{1,0:T(8,128)(2,1)S(1)} %collective-permute-done.2), channel_id=1, source_target_pairs={{0,1},{1,2},{2,3},{3,4},{4,5},{5,6},{6,7},{7,0},{8,9},{9,10},{10,1... | collective-permute-start | bytes 786440 | tf_op jit(solution)/shard_map/ppermute | solution.py:22
  171.6 7.9 %collective-permute-start.4 = (bf16[512,256]{1,0:T(8,128)(2,1)S(1)}, bf16[512,256]{1,0:T(8,128)(2,1)S(1)}, u32[]{:S(2)}, u32[]{:S(2)}) collective-permute-start(bf16[512,256]{1,0:T(8,128)(2,1)S(1)} %collective-permute-done.3), channel_id=1, source_target_pairs={{0,1},{1,2},{2,3},{3,4},{4,5},{5,6},{6,7},{7,0},{8,9},{9,10},{10,1... | collective-permute-start | bytes 786440 | tf_op jit(solution)/shard_map/ppermute | solution.py:22
  176.3 5.9 %copy-start.4 = (bf16[512,256]{1,0:T(8,128)(2,1)S(1)}, bf16[512,256]{1,0:T(8,128)(2,1)}, u32[]{:S(2)}) copy-start(bf16[512,256]{1,0:T(8,128)(2,1)} %copy-done.3) | copy-start | bytes 786436
  179.5 7.6 %collective-permute-start.5 = (bf16[512,256]{1,0:T(8,128)(2,1)S(1)}, bf16[512,256]{1,0:T(8,128)(2,1)S(1)}, u32[]{:S(2)}, u32[]{:S(2)}) collective-permute-start(bf16[512,256]{1,0:T(8,128)(2,1)S(1)} %collective-permute-done.4), channel_id=1, source_target_pairs={{0,1},{1,2},{2,3},{3,4},{4,5},{5,6},{6,7},{7,0},{8,9},{9,10},{10,1... | collective-permute-start | bytes 786440 | tf_op jit(solution)/shard_map/ppermute | solution.py:22
  187.1 7.6 %collective-permute-start.6 = (bf16[512,256]{1,0:T(8,128)(2,1)S(1)}, bf16[512,256]{1,0:T(8,128)(2,1)S(1)}, u32[]{:S(2)}, u32[]{:S(2)}) collective-permute-start(bf16[512,256]{1,0:T(8,128)(2,1)S(1)} %collective-permute-done.5), channel_id=1, source_target_pairs={{0,1},{1,2},{2,3},{3,4},{4,5},{5,6},{6,7},{7,0},{8,9},{9,10},{10,1... | collective-permute-start | bytes 786440 | tf_op jit(solution)/shard_map/ppermute | solution.py:22
  258.3 4.8 %copy-start = (bf16[2048,1024]{1,0:T(8,128)(2,1)S(1)}, bf16[2048,1024]{1,0:T(8,128)(2,1)}, u32[]{:S(2)}) copy-start(bf16[2048,1024]{1,0:T(8,128)(2,1)} %all-gather.6.cloned.1.call-done) | copy-start | bytes 12582916
Sparse Core Ops, SparseCore 0:
  10.4 55.2 all-gather.7
  68.2 52.5 all-gather.3
  123.2 52.5 all-gather.5
  217.8 40.4 reduce-scatter.1
